TPU v7x, 32 devices: a whole 2x2x4 slice. The times are simulated.
32 devices in a mesh: ep: 8 (over z, y), tp: 4 (over x, core).
Axes of the slice: x: 2, y: 2, z: 4, core: 2. Of those that a mesh axis runs over, the one named last changes fastest.
Arguments:
- tokens: bfloat16 [2048, 2048], P('ep', 'tp'), may hold values from -400 to 400
- expert_ids: int32 [2048, 2], P('ep'), may hold values from 0 to 7, all different within a row; in each aligned block of 256 rows (0 to 255, 256 to 511, ...) at most 80 rows name the same one
- route_weights: float32 [2048, 2], P('ep'), may hold values from 0.1 to 1
- pre_gain: float32 [2048], P('tp'), may hold values from 0.1 to 1.9
- post_gain: float32 [2048], P('tp'), may hold values from 0.1 to 1.9
- gate_weight: bfloat16 [8, 2048, 4096], P('ep', None, 'tp'), may hold values from -0.125 to 0.125
- up_weight: bfloat16 [8, 2048, 4096], P('ep', None, 'tp'), may hold values from -0.125 to 0.125
- down_weight: bfloat16 [8, 4096, 2048], P('ep', None, 'tp'), may hold values from -0.71875 to 0.71875
Outputs:
- layer_out: bfloat16 [2048, 2048], P('ep', 'tp')
Inputs may be any that keep to these rules, and one draw needn't show every extreme that they name: `expert_ids`: the 2 experts of a token are distinct. Within the rows of one device along ep, no expert is named more than 80 times, a bound that some block reaches.
All inputs are finite; a program needn't handle non-finite values.
Results may differ from a plain program's by a relative error of at most 0.007.
Values may be sent and summed in bfloat16 or wider, within the bound.
A program may use at most 64 MiB of HBM per device.

v0:
```python
import jax
import jax.numpy as jnp
from jax import lax
from jax.sharding import PartitionSpec as P

epsilon = 1e-06


def on_device(
    tokens, expert_ids, route_weights, pre_gain, post_gain, gate_weight, up_weight, down_weight
):
    tok_rows, width_part = tokens.shape
    width_full = width_part * lax.axis_size("tp")
    ep_count = lax.axis_size("ep")
    local_count = gate_weight.shape[0]
    experts_all = local_count * ep_count
    top_count = expert_ids.shape[1]
    capacity = max(2, tok_rows * top_count * 5 // (4 * experts_all))
    slot_total = experts_all * capacity
    tok_float = tokens.astype(jnp.float32)
    square_sum = lax.psum(jnp.sum(tok_float * tok_float, axis=1), "tp")
    inv_scale = lax.rsqrt(square_sum / width_full + epsilon)
    normed = (tok_float * inv_scale[:, None] * pre_gain[None, :]).astype(jnp.bfloat16)
    flat_ids = expert_ids.reshape(-1)
    onehot = (flat_ids[:, None] == jnp.arange(experts_all, dtype=jnp.int32)[None, :]).astype(
        jnp.int32
    )
    slot = jnp.sum((jnp.cumsum(onehot, axis=0) - 1) * onehot, axis=1)
    target = (flat_ids * capacity + slot).reshape(tok_rows, top_count)
    slot_index = jnp.arange(slot_total, dtype=jnp.int32)
    pick_map = (jnp.transpose(target).reshape(-1)[:, None] == slot_index[None, :]).astype(
        jnp.bfloat16
    )
    dispatch_map = jnp.sum(pick_map.reshape(top_count, tok_rows, slot_total), axis=0)
    outgoing = jnp.dot(
        jnp.transpose(dispatch_map), normed, preferred_element_type=jnp.float32
    ).astype(jnp.bfloat16)
    outgoing = outgoing.reshape(ep_count, local_count, capacity, width_part)
    arrived = lax.all_to_all(outgoing, "ep", split_axis=0, concat_axis=2, tiled=True)
    arrived = arrived.reshape(local_count, ep_count * capacity, width_part)
    row_total = ep_count * capacity
    features = lax.all_gather(arrived, "tp", axis=2, tiled=True)
    gate = jnp.einsum("erd,edh->erh", features, gate_weight, preferred_element_type=jnp.float32)
    upper = jnp.einsum("erd,edh->erh", features, up_weight, preferred_element_type=jnp.float32)
    hidden = (jax.nn.silu(gate) * upper).astype(jnp.bfloat16)
    hidden_whole = lax.all_gather(hidden, "tp", axis=2, tiled=True)
    result = jnp.einsum(
        "erh,ehd->erd", hidden_whole, down_weight, preferred_element_type=jnp.float32
    )
    expert_out = result.astype(jnp.bfloat16).reshape(1, local_count, row_total, width_part)
    returned = lax.all_to_all(expert_out, "ep", split_axis=2, concat_axis=0, tiled=True)
    returned = returned.reshape(slot_total, width_part)
    picked = jnp.dot(pick_map, returned, preferred_element_type=jnp.float32).reshape(
        top_count, tok_rows, width_part
    )
    mixed = jnp.sum(picked * jnp.transpose(route_weights)[:, :, None], axis=0)
    out_sum = lax.psum(jnp.sum(mixed * mixed, axis=1), "tp")
    out_scale = lax.rsqrt(out_sum / width_full + epsilon)
    return (mixed * out_scale[:, None] * post_gain[None, :]).astype(jnp.bfloat16)


def solution(mesh):
    return jax.shard_map(
        on_device,
        mesh=mesh,
        in_specs=(
            P("ep", "tp"),
            P("ep", None),
            P("ep", None),
            P("tp"),
            P("tp"),
            P("ep", None, "tp"),
            P("ep", None, "tp"),
            P("ep", None, "tp"),
        ),
        out_specs=P("ep", "tp"),
        check_vma=False,
    )
```

profile of v0, /device:TPU:0, one launch (start us, length us, event | category | flops | bytes accessed | tf_op | source)
XLA Modules:
  0.0 170.0 jit_solution(17323781832735627482)
XLA Ops:
  6.5 0.8 copy.39
  7.4 0.1 eq.65
  7.5 0.1 eq.61
  7.7 1.1 reduce-window.6
  8.8 0.2 slice_reduce_fusion
  9.1 0.1 fusion.34
  9.2 0.1 reduce_sum.51
  9.3 0.1 copy.41
  9.4 0.7 add_bitcast_fusion
  10.1 0.2 fusion.24
  10.3 1.1 fusion.28
  11.4 8.4 %psum.14 = f32[256]{0:T(256)S(1)} all-reduce(f32[256]{0:T(256)S(1)} %fusion.28), channel_id=1, replica_groups=mesh['ep'=8,'tp'=4] {'tp'}, use_global_device_ids=true, to_apply=%region_5.6 | all-reduce | flops 256 | bytes 2048 | tf_op jit(solution)/shard_map/psum | solution.py:21
  19.7 1.4 convolution_convert_fusion
  21.1 22.2 %all_to_all.8 = bf16[8,1,80,512]{3,2,1,0:T(8,128)(2,1)} all-to-all(bf16[8,1,80,512]{3,2,1,0:T(8,128)(2,1)S(1)} %bitcast.53), channel_id=1, replica_groups=mesh['ep'=8,'tp'=4] {'ep'}, dimensions={0} | all-to-all | bytes 1310720 | tf_op jit(solution)/shard_map/all_to_all | solution.py:39
  43.3 0.0 all-gather.4.cloned.1.call-update
  43.4 0.0 all-gather.6.cloned.1.call-start
  43.4 24.3 %all-gather.4.cloned.1.call-done = bf16[1,640,2048]{2,1,0:T(8,128)(2,1)} async-done(((bf16[1,640,512]{2,1,0:T(8,128)(2,1)}), bf16[1,640,2048]{2,1,0:T(8,128)(2,1)}) %all-gather.4.cloned.1.call-update) | async-done | bytes 2621456 | tf_op jit(solution)/shard_map/all_gather | solution.py:42
  67.8 5.6 %fusion.4 = f32[640,1024]{1,0:T(8,128)S(1)} fusion(bf16[1,2048,1024]{2,1,0:T(8,128)(2,1)} %param.13, bf16[1,640,2048]{2,1,0:T(8,128)(2,1)} %all-gather.4.cloned.1.call-done), kind=kOutput, calls=%fused_computation.4 | convolution fusion | flops 2684354560 | bytes 9437184 | tf_op jit(solution)/shard_map/erd,edh->erh/dot_general | solution.py:43
  73.4 4.2 %multiply_convert_fusion = bf16[640,1024]{1,0:T(8,128)(2,1)} fusion(f32[640,1024]{1,0:T(8,128)S(1)} %fusion.4, bf16[1,2048,1024]{2,1,0:T(8,128)(2,1)S(1)} %copy-done.1, bf16[1,640,2048]{2,1,0:T(8,128)(2,1)S(1)} %copy-done.2), kind=kOutput, calls=%fused_computation.8 | convolution fusion | flops 2688286720 | bytes 10747904 | tf_op jit(solution)/shard_map/erd,edh->erh/dot_general | solution.py:44
  77.6 0.0 all-gather.6.cloned.1.call-update
  77.6 40.6 %all-gather.6.cloned.1.call-done = bf16[640,4096]{1,0:T(8,128)(2,1)} async-done(((bf16[640,1024]{1,0:T(8,128)(2,1)}), bf16[640,4096]{1,0:T(8,128)(2,1)}) %all-gather.6.cloned.1.call-update) | async-done | bytes 5242896 | tf_op jit(solution)/shard_map/all_gather | solution.py:46
  118.2 6.6 %fusion.21 = bf16[1,1,640,512]{3,2,1,0:T(8,128)(2,1)S(1)} fusion(bf16[640,4096]{1,0:T(8,128)(2,1)} %all-gather.6.cloned.1.call-done, bf16[1,4096,512]{2,1,0:T(8,128)(2,1)} %param.15), kind=kOutput, calls=%fused_computation.17 | convolution fusion | flops 2684682240 | bytes 10092544 | tf_op jit(solution)/shard_map/erh,ehd->erd/dot_general | solution.py:47
  124.8 1.0 copy.50
  125.8 0.5 broadcast.77
  126.3 4.8 %reduce.3 = bf16[640,512]{1,0:T(8,128)(2,1)S(1)} reduce(bf16[640,1,1,512]{3,2,1,0:T(2,128)(2,1)S(1)} %bitcast.51, bf16[]{:T(256)} %broadcast.77), dimensions={1,2}, to_apply=%bitcast.50.reduce_sub_computation | reduce | bytes 1310722
  131.1 0.5 reshape.125
  131.6 23.4 %all_to_all.9 = bf16[8,2,20480]{2,1,0:T(2,128)(2,1)S(1)} all-to-all(bf16[8,2,20480]{2,1,0:T(2,128)(2,1)S(1)} %reshape.125), channel_id=1, replica_groups=mesh['ep'=8,'tp'=4] {'ep'}, dimensions={0} | all-to-all | bytes 1310720 | tf_op jit(solution)/shard_map/all_to_all | solution.py:51
  155.0 0.6 reshape.126
  155.6 0.6 fusion.18
  156.3 0.1 multiply_reduce_fusion
  156.4 6.0 %psum.15 = f32[256]{0:T(256)S(1)} all-reduce(f32[256]{0:T(256)S(1)} %multiply_reduce_fusion), channel_id=1, replica_groups=mesh['ep'=8,'tp'=4] {'tp'}, use_global_device_ids=true, to_apply=%region_8.9 | all-reduce | flops 256 | bytes 2048 | tf_op jit(solution)/shard_map/psum | solution.py:57
  162.4 0.8 multiply_convert_fusion.1
  (14 shorter events, 0.1 us)
Async XLA Ops:
  6.5 61.2 %all-gather.4.cloned.1.call-start = ((), (), s32[]{:S(2)}) async-start(), calls=%async_computation.2 | async-start | bytes 3276800 | tf_op jit(solution)/shard_map/all_gather | solution.py:42
  43.4 74.8 %all-gather.6.cloned.1.call-start = ((), (), s32[]{:S(2)}) async-start(), calls=%async_computation.3 | async-start | bytes 6553600 | tf_op jit(solution)/shard_map/all_gather | solution.py:46
  67.8 5.6 %copy-start.1 = (bf16[1,2048,1024]{2,1,0:T(8,128)(2,1)S(1)}, bf16[1,2048,1024]{2,1,0:T(8,128)(2,1)}, u32[]{:S(2)}) copy-start(bf16[1,2048,1024]{2,1,0:T(8,128)(2,1)} %param.14) | copy-start | bytes 12582916
  67.8 5.6 %copy-start.2 = (bf16[1,640,2048]{2,1,0:T(8,128)(2,1)S(1)}, bf16[1,640,2048]{2,1,0:T(8,128)(2,1)}, u32[]{:S(2)}) copy-start(bf16[1,640,2048]{2,1,0:T(8,128)(2,1)} %all-gather.4.cloned.1.call-done) | copy-start | bytes 7864324
  131.1 24.5 %copy-start.3 = (f32[256,2]{0,1:T(2,128)S(1)}, f32[256,2]{0,1:T(2,128)}, u32[]{:S(2)}) copy-start(f32[256,2]{0,1:T(2,128)} %param.10) | copy-start | bytes 6148
  155.0 7.4 %copy-start = (f32[512]{0:T(512)S(1)}, f32[512]{0:T(512)}, u32[]{:S(2)}) copy-start(f32[512]{0:T(512)} %param.12) | copy-start | bytes 6148
Sparse Core Ops, SparseCore 0:
  43.5 24.2 all-gather.3
  77.7 40.3 all-gather.5
where the time goes:
time: 170 us
  waiting for transfers between devices  64.9 us (38%)
  blocking collectives  59.9 us (35%)
  matrix products  18.4 us (11%)
  between operations  13.5 us (8%)
  other arithmetic  8.99 us (5%)
  local copies, waits for them, and re-layouts  4.19 us (2%)
    all_gather x1, waiting for transfers between devices, on_device(): hidden_whole = lax.all_gather(hidden, 'tp', axis=2, tiled=True)  40.6 us
    all_gather x1, waiting for transfers between devices, on_device(): features = lax.all_gather(arrived, 'tp', axis=2, tiled=True)  24.3 us
    all_to_all x1, blocking collectives, on_device(): lax.all_to_all(expert_out, 'ep', split_axis=2, concat_axis=0, tiled=True)  23.4 us
    all_to_all x1, blocking collectives, on_device(): lax.all_to_all(outgoing, 'ep', split_axis=0, concat_axis=2, tiled=True)  22.2 us
    psum x1, blocking collectives, on_device(): square_sum = lax.psum(jnp.sum(tok_float * tok_float, axis=1), 'tp')  8.37 us
    dot_general x1, matrix products, on_device(): jnp.einsum('erh,ehd->erd', hidden_whole, down_weight, preferred_element_t...  6.62 us
    psum x1, blocking collectives, on_device(): out_sum = lax.psum(jnp.sum(mixed * mixed, axis=1), 'tp')  5.95 us
    dot_general x1, matrix products, on_device(): jnp.einsum('erd,edh->erh', features, gate_weight, preferred_element_type=...  5.58 us
  transfers between devices with their start and end apart: 2, of which 2 were waited for; matrix products, arithmetic and copies ran while one was open for 0% of the time, Pallas kernels for 0%

commit v1 on v0

--- a/solution.py
+++ b/solution.py
@@ -43,10 +43,38 @@
     gate = jnp.einsum("erd,edh->erh", features, gate_weight, preferred_element_type=jnp.float32)
     upper = jnp.einsum("erd,edh->erh", features, up_weight, preferred_element_type=jnp.float32)
     hidden = (jax.nn.silu(gate) * upper).astype(jnp.bfloat16)
-    hidden_whole = lax.all_gather(hidden, "tp", axis=2, tiled=True)
-    result = jnp.einsum(
-        "erh,ehd->erd", hidden_whole, down_weight, preferred_element_type=jnp.float32
+    size, place, span = (lax.axis_size("tp"), lax.axis_index("tp"), hidden.shape[2])
+    right = [(i, (i + 1) % size) for i in range(size)]
+    downward = [(i, (i - 1) % size) for i in range(size)]
+    half = size // 2
+    from_left = from_right = hidden
+    total = jnp.einsum(
+        "erh,ehd->erd",
+        hidden,
+        lax.dynamic_slice_in_dim(down_weight, place * span, hidden.shape[2], axis=1),
+        preferred_element_type=jnp.float32,
     )
+    for turn in range(1, half + 1):
+        from_left = lax.ppermute(from_left, "tp", right)
+        if turn < size - half:
+            from_right = lax.ppermute(from_right, "tp", downward)
+            total = total + jnp.einsum(
+                "erh,ehd->erd",
+                from_right,
+                lax.dynamic_slice_in_dim(
+                    down_weight, (place + turn) % size * span, from_right.shape[2], axis=1
+                ),
+                preferred_element_type=jnp.float32,
+            )
+        total = total + jnp.einsum(
+            "erh,ehd->erd",
+            from_left,
+            lax.dynamic_slice_in_dim(
+                down_weight, (place - turn) % size * span, from_left.shape[2], axis=1
+            ),
+            preferred_element_type=jnp.float32,
+        )
+    result = total
     expert_out = result.astype(jnp.bfloat16).reshape(1, local_count, row_total, width_part)
     returned = lax.all_to_all(expert_out, "ep", split_axis=2, concat_axis=0, tiled=True)
     returned = returned.reshape(slot_total, width_part)

time: 170 us -> 168 us (0.988)
  blocking collectives: 59.9 us -> 56.6 us
  starting transfers between devices: 0.04 us -> 1.8 us
    all_gather x1 -> x0, waiting for transfers between devices: 40.6 us -> none  [on_device(): hidden_whole = lax.all_gather(hidden, 'tp', axis=2, tiled=True)]
    ppermute x0 -> x3, waiting for transfers between devices: none -> 40.3 us  [the longest x2 40.3 us: on_device(): from_left = lax.ppermute(from_left, 'tp', right)]
    all_to_all x1, blocking collectives: 23.4 us -> 20.1 us  [on_device(): lax.all_to_all(expert_out, 'ep', split_axis=2, concat_axis=0, tiled=True)]
    ppermute x0 -> x3, starting transfers between devices: none -> 1.8 us  [the longest x1 1.51 us: on_device(): from_right = lax.ppermute(from_right, 'tp', downward)]
    dot_general x1 -> x4, matrix products: 6.62 us -> 7.39 us  [the longest x2 3.02 us: on_device(): jnp.einsum('erh,ehd->erd', from_left, lax.dynamic_slice_in_dim(down_weigh...]
  transfers between devices with their start and end apart: 2 -> 4, of which waited for: 2 -> 3; matrix products, arithmetic and copies ran while one was open for 0% -> 3% of each run, Pallas kernels for 0% -> 0%
where the time goes in v1:
time: 168 us; the launch traced here: 167 us
  waiting for transfers between devices  64.7 us (39%)
  blocking collectives  56.6 us (34%)
  matrix products  17.1 us (10%)
  between operations  13.5 us (8%)
  other arithmetic  8.99 us (5%)
  local copies, waits for them, and re-layouts  4.54 us (3%)
  starting transfers between devices  1.8 us (1%)
    ppermute x2, waiting for transfers between devices, on_device(): from_left = lax.ppermute(from_left, 'tp', right)  40.3 us
    all_gather x1, waiting for transfers between devices, on_device(): features = lax.all_gather(arrived, 'tp', axis=2, tiled=True)  24.4 us
    all_to_all x1, blocking collectives, on_device(): lax.all_to_all(outgoing, 'ep', split_axis=0, concat_axis=2, tiled=True)  22.2 us
    all_to_all x1, blocking collectives, on_device(): lax.all_to_all(expert_out, 'ep', split_axis=2, concat_axis=0, tiled=True)  20.1 us
    psum x1, blocking collectives, on_device(): square_sum = lax.psum(jnp.sum(tok_float * tok_float, axis=1), 'tp')  8.37 us
    psum x1, blocking collectives, on_device(): out_sum = lax.psum(jnp.sum(mixed * mixed, axis=1), 'tp')  5.94 us
    dot_general x1, matrix products, on_device(): jnp.einsum('erd,edh->erh', features, gate_weight, preferred_element_type=...  5.58 us
    unnamed x1, other arithmetic  4.79 us
  transfers between devices with their start and end apart: 4, of which 3 were waited for; matrix products, arithmetic and copies ran while one was open for 3% of the time, Pallas kernels for 0%

profile of v1, /device:TPU:0, one launch (start us, length us, event | category | flops | bytes accessed | tf_op | source)
XLA Modules:
  0.0 167.3 jit_solution(6720261649194700914)
XLA Ops:
  6.5 0.8 copy.39
  7.4 0.1 eq.69
  7.7 1.1 reduce-window.6
  8.8 0.2 slice_reduce_fusion
  9.2 0.1 reduce_sum.51
  9.4 0.7 add_bitcast_fusion
  10.1 0.2 fusion.32
  10.3 1.1 fusion.36
  11.4 8.4 %psum.14 = f32[256]{0:T(256)S(1)} all-reduce(f32[256]{0:T(256)S(1)} %fusion.36), channel_id=1, replica_groups=mesh['ep'=8,'tp'=4] {'tp'}, use_global_device_ids=true, to_apply=%region_5.6 | all-reduce | flops 256 | bytes 2048 | tf_op jit(solution)/shard_map/psum | solution.py:21
  19.8 0.4 convolution_convert_fusion
  20.2 22.2 %all_to_all.8 = bf16[8,1,80,512]{3,2,1,0:T(8,128)(2,1)} all-to-all(bf16[8,1,80,512]{3,2,1,0:T(8,128)(2,1)S(1)} %bitcast.70), channel_id=1, replica_groups=mesh['ep'=8,'tp'=4] {'ep'}, dimensions={0} | all-to-all | bytes 1310720 | tf_op jit(solution)/shard_map/all_to_all | solution.py:39
  42.5 24.4 %all-gather.2.cloned.1.call-done = bf16[1,640,2048]{2,1,0:T(8,128)(2,1)} async-done(((bf16[1,640,512]{2,1,0:T(8,128)(2,1)}), bf16[1,640,2048]{2,1,0:T(8,128)(2,1)}) %all-gather.2.cloned.1.call-update) | async-done | bytes 2621456 | tf_op jit(solution)/shard_map/all_gather | solution.py:42
  66.9 5.6 %fusion.2 = f32[640,1024]{1,0:T(8,128)S(1)} fusion(bf16[1,2048,1024]{2,1,0:T(8,128)(2,1)} %param.13, bf16[1,640,2048]{2,1,0:T(8,128)(2,1)} %all-gather.2.cloned.1.call-done), kind=kOutput, calls=%fused_computation.2 | convolution fusion | flops 2684354560 | bytes 9437184 | tf_op jit(solution)/shard_map/erd,edh->erh/dot_general | solution.py:43
  72.5 3.1 %multiply_convert_fusion = bf16[640,1024]{1,0:T(8,128)(2,1)S(1)} fusion(f32[640,1024]{1,0:T(8,128)S(1)} %fusion.2, bf16[1,2048,1024]{2,1,0:T(8,128)(2,1)S(1)} %copy-done.3, bf16[1,640,2048]{2,1,0:T(8,128)(2,1)S(1)} %copy-done.5), kind=kOutput, calls=%fused_computation.6 | convolution fusion | flops 2688286720 | bytes 10747904 | tf_op jit(solution)/shard_map/erd,edh->erh/dot_general | solution.py:44
  75.6 0.3 collective-permute-start.1
  75.9 1.5 collective-permute-start
  77.4 28.7 %collective-permute-done.1 = bf16[1,640,1024]{2,1,0:T(8,128)(2,1)S(1)} collective-permute-done((bf16[1,640,1024]{2,1,0:T(8,128)(2,1)S(1)}, bf16[1,640,1024]{2,1,0:T(8,128)(2,1)S(1)}, u32[]{:S(2)}, u32[]{:S(2)}) %collective-permute-start.1) | collective-permute-done | bytes 1310752 | tf_op jit(solution)/shard_map/ppermute | solution.py:58
  106.1 2.2 %fusion.26 = f32[640,512]{1,0:T(8,128)S(1)} fusion(bf16[640,1024]{1,0:T(8,128)(2,1)S(1)} %multiply_convert_fusion, bf16[1,4096,512]{2,1,0:T(8,128)(2,1)} %param.15, s32[]{:T(128)S(6)} %select_n.27), kind=kOutput, calls=%fused_computation.25 | convolution fusion | flops 671088640 | bytes 3670020 | tf_op jit(solution)/shard_map/erh,ehd->erd/dot_general | solution.py:51
  108.3 0.3 copy-done.4
  108.6 2.2 %convolution_add_fusion.2 = f32[640,512]{1,0:T(8,128)S(1)} fusion(f32[640,512]{1,0:T(8,128)S(1)} %fusion.26, bf16[1,640,1024]{2,1,0:T(8,128)(2,1)} %collective-permute-done, bf16[1,4096,512]{2,1,0:T(8,128)(2,1)S(1)} %copy-done.4, s32[]{:T(128)S(6)} %select_n.29), kind=kOutput, calls=%fused_computation.9 | convolution fusion | flops 671416320 | bytes 4980740 | tf_op jit(solution)/shard_map/erh,ehd->erd/dot_general | solution.py:61
  110.7 0.9 convolution_add_fusion.1
  111.6 11.6 %collective-permute-done.2 = bf16[1,640,1024]{2,1,0:T(8,128)(2,1)} collective-permute-done((bf16[1,640,1024]{2,1,0:T(8,128)(2,1)S(1)}, bf16[1,640,1024]{2,1,0:T(8,128)(2,1)}, u32[]{:S(2)}, u32[]{:S(2)}) %collective-permute-start.2) | collective-permute-done | bytes 1310752 | tf_op jit(solution)/shard_map/ppermute | solution.py:58
  123.2 2.2 %fusion.20 = bf16[1,1,640,512]{3,2,1,0:T(8,128)(2,1)S(1)} fusion(f32[640,512]{1,0:T(8,128)S(1)} %convolution_add_fusion.1, bf16[1,640,1024]{2,1,0:T(8,128)(2,1)} %collective-permute-done.2, bf16[1,4096,512]{2,1,0:T(8,128)(2,1)S(1)} %copy-done.4, s32[]{:T(128)S(6)} %select_n.33), kind=kOutput, calls=%fused_computation.21 | convolution fusion | flops 671744000 | bytes 4325380 | tf_op jit(solution)/shard_map/erh,ehd->erd/dot_general | solution.py:69
  125.4 1.0 copy.50
  126.4 0.5 broadcast.80
  126.9 4.8 %reduce.3 = bf16[640,512]{1,0:T(8,128)(2,1)S(1)} reduce(bf16[640,1,1,512]{3,2,1,0:T(2,128)(2,1)S(1)} %bitcast.68, bf16[]{:T(256)} %broadcast.80), dimensions={1,2}, to_apply=%bitcast.67.reduce_sub_computation | reduce | bytes 1310722
  131.7 0.5 reshape.151
  132.2 20.1 %all_to_all.9 = bf16[8,2,20480]{2,1,0:T(2,128)(2,1)S(1)} all-to-all(bf16[8,2,20480]{2,1,0:T(2,128)(2,1)S(1)} %reshape.151), channel_id=1, replica_groups=mesh['ep'=8,'tp'=4] {'ep'}, dimensions={0} | all-to-all | bytes 1310720 | tf_op jit(solution)/shard_map/all_to_all | solution.py:79
  152.3 0.6 reshape.152
  153.0 0.6 fusion.17
  153.7 5.9 %psum.15 = f32[256]{0:T(256)S(1)} all-reduce(f32[256]{0:T(256)S(1)} %multiply_reduce_fusion), channel_id=1, replica_groups=mesh['ep'=8,'tp'=4] {'tp'}, use_global_device_ids=true, to_apply=%region_8.9 | all-reduce | flops 256 | bytes 2048 | tf_op jit(solution)/shard_map/psum | solution.py:85
  159.7 0.8 multiply_convert_fusion.1
  (26 shorter events, 0.6 us)
Async XLA Ops:
  6.5 13.2 %copy-start = (bf16[256,512]{1,0:T(8,128)(2,1)S(1)}, bf16[256,512]{1,0:T(8,128)(2,1)}, u32[]{:S(2)}) copy-start(bf16[256,512]{1,0:T(8,128)(2,1)} %param.8) | copy-start | bytes 786436
  6.5 13.2 %copy-start.1 = (f32[512]{0:T(512)S(1)}, f32[512]{0:T(512)}, u32[]{:S(2)}) copy-start(f32[512]{0:T(512)} %param.11) | copy-start | bytes 6148
  6.5 60.3 %all-gather.2.cloned.1.call-start = ((), (), s32[]{:S(2)}) async-start(), calls=%async_computation.2 | async-start | bytes 3276800 | tf_op jit(solution)/shard_map/all_gather | solution.py:42
  66.9 5.6 %copy-start.3 = (bf16[1,2048,1024]{2,1,0:T(8,128)(2,1)S(1)}, bf16[1,2048,1024]{2,1,0:T(8,128)(2,1)}, u32[]{:S(2)}) copy-start(bf16[1,2048,1024]{2,1,0:T(8,128)(2,1)} %param.14) | copy-start | bytes 12582916
  66.9 5.6 %copy-start.5 = (bf16[1,640,2048]{2,1,0:T(8,128)(2,1)S(1)}, bf16[1,640,2048]{2,1,0:T(8,128)(2,1)}, u32[]{:S(2)}) copy-start(bf16[1,640,2048]{2,1,0:T(8,128)(2,1)} %all-gather.2.cloned.1.call-done) | copy-start | bytes 7864324
  75.6 30.5 %collective-permute-start.1 = (bf16[1,640,1024]{2,1,0:T(8,128)(2,1)S(1)}, bf16[1,640,1024]{2,1,0:T(8,128)(2,1)S(1)}, u32[]{:S(2)}, u32[]{:S(2)}) collective-permute-start(bf16[1,640,1024]{2,1,0:T(8,128)(2,1)S(1)} %bitcast.72), channel_id=1, source_target_pairs={{0,1},{1,2},{2,3},{3,0},{4,5},{5,6},{6,7},{7,4},{8,9},{9,10},{10,1... | collective-permute-start | bytes 3932168 | tf_op jit(solution)/shard_map/ppermute | solution.py:58
  75.9 32.4 %collective-permute-start = (bf16[1,640,1024]{2,1,0:T(8,128)(2,1)S(1)}, bf16[1,640,1024]{2,1,0:T(8,128)(2,1)}, u32[]{:S(2)}, u32[]{:S(2)}) collective-permute-start(bf16[1,640,1024]{2,1,0:T(8,128)(2,1)S(1)} %bitcast.73), channel_id=1, source_target_pairs={{0,3},{1,0},{2,1},{3,2},{4,7},{5,4},{6,5},{7,6},{8,11},{9,8},{10,9... | collective-permute-start | bytes 3932168 | tf_op jit(solution)/shard_map/ppermute | solution.py:60
  106.1 17.1 %collective-permute-start.2 = (bf16[1,640,1024]{2,1,0:T(8,128)(2,1)S(1)}, bf16[1,640,1024]{2,1,0:T(8,128)(2,1)}, u32[]{:S(2)}, u32[]{:S(2)}) collective-permute-start(bf16[1,640,1024]{2,1,0:T(8,128)(2,1)S(1)} %collective-permute-done.1), channel_id=1, source_target_pairs={{0,1},{1,2},{2,3},{3,0},{4,5},{5,6},{6,7},{7,4},{8,9},{9,10},{10,1... | collective-permute-start | bytes 3932168 | tf_op jit(solution)/shard_map/ppermute | solution.py:58
  106.1 2.5 %copy-start.4 = (bf16[1,4096,512]{2,1,0:T(8,128)(2,1)S(1)}, bf16[1,4096,512]{2,1,0:T(8,128)(2,1)}, u32[]{:S(2)}) copy-start(bf16[1,4096,512]{2,1,0:T(8,128)(2,1)} %param.15) | copy-start | bytes 12582916
  152.3 0.7 copy-start.6
  153.0 6.7 %copy-start.2 = (f32[512]{0:T(512)S(1)}, f32[512]{0:T(512)}, u32[]{:S(2)}) copy-start(f32[512]{0:T(512)} %param.12) | copy-start | bytes 6148
Sparse Core Ops, SparseCore 0:
  42.6 24.2 all-gather.1
